TPU v7x, 256 devices: a whole 4x4x8 slice. The times are simulated.
256 devices in a mesh: fs: 64 (over z, y, core), tp: 4 (over x).
Axes of the slice: x: 4, y: 4, z: 8, core: 2. Of those that a mesh axis runs over, the one named last changes fastest.
Arguments:
- later_gate: bfloat16 [40960, 5632], P('fs', 'tp'), may hold values from -6 to 6
- later_up: bfloat16 [40960, 5632], P('fs', 'tp'), may hold values from -6 to 6
- early_gate: bfloat16 [40960, 5632], P('fs', 'tp'), may hold values from -6 to 6
- early_up: bfloat16 [40960, 5632], P('fs', 'tp'), may hold values from -6 to 6
- early_cotangent: bfloat16 [40960, 2048], P(('fs', 'tp')), may hold values from -24 to 24
- down_weight: bfloat16 [5632, 2048], P('tp', 'fs'), may hold values from -0.078125 to 0.078125
- grad_running: float32 [5632, 2048], P('tp', 'fs'), may hold values from -640 to 640
Outputs:
- mixed: bfloat16 [40960, 2048], P(('fs', 'tp'))
- gate_grad: bfloat16 [40960, 5632], P('fs', 'tp')
- up_grad: bfloat16 [40960, 5632], P('fs', 'tp')
- grad_total: float32 [5632, 2048], P('tp', 'fs')
All inputs are finite; a program needn't handle non-finite values.
Results may differ from a plain program's by a relative error of at most 0.009.
Values may be sent and summed in bfloat16 or wider, within the bound.
A program may use at most 128 MiB of HBM per device.

v0:
```python
import jax
import jax.numpy as jnp
from jax import lax
from jax.sharding import PartitionSpec as P


def laid_out(tiles, dim):
    dims = list(tiles.shape[1:])
    dims[dim] *= tiles.shape[0]
    return jnp.moveaxis(tiles, 0, dim).reshape(dims)


def copy_for_each(x, axis):
    size = lax.axis_size(axis)
    return lax.all_to_all(jnp.broadcast_to(x[None], (size, *x.shape)), axis, 0, 0, tiled=True)


def gather_directly(x, axis, dim):
    return laid_out(copy_for_each(x, axis), dim)


def cut_along(x, dim, size):
    before, after = (x.shape[:dim], x.shape[dim + 1 :])
    return jnp.moveaxis(x.reshape(*before, size, -1, *after), dim, 0)


def sent_and_summed(x, axis, dim):
    tiles = cut_along(x, dim, lax.axis_size(axis))
    arrived = lax.all_to_all(tiles, axis, split_axis=0, concat_axis=0, tiled=True)
    return arrived.astype(jnp.float32).sum(axis=0)


def on_device(
    later_gate, later_up, early_gate, early_up, early_cotangent, down_weight, grad_running
):
    later_hidden = (
        jax.nn.silu(later_gate.astype(jnp.float32)) * later_up.astype(jnp.float32)
    ).astype(jnp.bfloat16)
    gate_value = early_gate.astype(jnp.float32)
    up_value = early_up.astype(jnp.float32)
    sigma = jax.nn.sigmoid(gate_value)
    early_hidden = (gate_value * sigma * up_value).astype(jnp.bfloat16)
    cot_rows = gather_directly(early_cotangent, "tp", 0)
    whole = lax.all_gather(down_weight, "fs", axis=1, tiled=True)
    mixed = sent_and_summed(
        jnp.dot(later_hidden, whole, preferred_element_type=jnp.float32).astype(jnp.bfloat16),
        "tp",
        0,
    ).astype(jnp.bfloat16)
    hidden_cot = lax.dot_general(
        cot_rows, whole, (((1,), (1,)), ((), ())), preferred_element_type=jnp.float32
    )
    gate_grad = (hidden_cot * up_value * sigma * (1.0 + gate_value * (1.0 - sigma))).astype(
        jnp.bfloat16
    )
    up_grad = (hidden_cot * gate_value * sigma).astype(jnp.bfloat16)
    summed = lax.psum_scatter(
        lax.dot_general(
            cot_rows, early_hidden, (((0,), (0,)), ((), ())), preferred_element_type=jnp.float32
        ),
        "fs",
        scatter_dimension=0,
        tiled=True,
    )
    grad_total = grad_running + summed.T
    return (mixed, gate_grad, up_grad, grad_total)


def solution(mesh):
    placed = (
        P("fs", "tp"),
        P("fs", "tp"),
        P("fs", "tp"),
        P("fs", "tp"),
        P(("fs", "tp"), None),
        P("tp", "fs"),
        P("tp", "fs"),
    )
    return jax.shard_map(
        on_device,
        mesh=mesh,
        in_specs=placed,
        out_specs=(P(("fs", "tp"), None), P("fs", "tp"), P("fs", "tp"), P("tp", "fs")),
        check_vma=False,
    )
```

profile of v0, /device:TPU:1, one launch (start us, length us, event | category | flops | bytes accessed | tf_op | source)
XLA Modules:
  0.0 259.6 jit_solution(15338845092056595441)
XLA Ops:
  7.2 0.0 all-gather.2.cloned.1.call-start
  7.2 0.7 all-gather.2.cloned.1.call-update
  7.9 0.0 copy-start.3
  7.9 0.0 reduce-scatter.4.cloned.1.call-start
  8.0 0.0 copy-start.4
  8.0 1.5 broadcast_in_dim.2
  9.5 35.6 %all_to_all.10 = bf16[4,160,2048]{2,1,0:T(8,128)(2,1)S(1)} all-to-all(bf16[4,160,2048]{2,1,0:T(8,128)(2,1)S(1)} %broadcast_in_dim.2), channel_id=1, replica_groups=mesh['fs'=64,'tp'=4] {'tp'}, dimensions={0} | all-to-all | bytes 5242880 | tf_op jit(solution)/shard_map/all_to_all | solution.py:15
  45.1 0.0 copy-start
  45.1 1.5 copy-done
  46.6 0.0 copy-done.3
  46.7 0.0 copy-done.4
  46.7 7.9 %convolution_bitcast_fusion = f32[2048,1408]{0,1:T(8,128)} fusion(bf16[640,2048]{1,0:T(8,128)(2,1)S(1)} %bitcast.11, bf16[640,1408]{1,0:T(8,128)(2,1)S(1)} %copy-done.4, bf16[640,1408]{1,0:T(8,128)(2,1)S(1)} %copy-done.3), kind=kOutput, calls=%fused_computation | convolution fusion | flops 3698196480 | bytes 17760256 | tf_op jit(solution)/shard_map/dot_general | solution.py:58
  54.5 12.1 %copy.15 = f32[2048,1408]{1,0:T(8,128)} copy(f32[2048,1408]{0,1:T(8,128)} %convolution_bitcast_fusion) | data formatting | bytes 23068672
  66.6 0.0 copy-start.2
  66.6 0.0 reduce-scatter.4.cloned.1.call-update
  66.7 28.3 %all-gather.2.cloned.1.call-done = bf16[1408,2048]{0,1:T(8,128)(2,1)} async-done(((bf16[1408,32]{0,1:T(8,128)(2,1)}), bf16[1408,2048]{0,1:T(8,128)(2,1)}) %all-gather.2.cloned.1.call-update) | async-done | bytes 5767184 | tf_op jit(solution)/shard_map/all_gather | solution.py:44
  95.0 0.0 copy-done.2
  95.0 9.2 %convolution_convert_fusion = bf16[640,2048]{1,0:T(8,128)(2,1)} fusion(bf16[1408,2048]{0,1:T(8,128)(2,1)} %all-gather.2.cloned.1.call-done, bf16[640,1408]{1,0:T(8,128)(2,1)S(1)} %copy-done.2, bf16[640,1408]{1,0:T(8,128)(2,1)} %param.7), kind=kOutput, calls=%fused_computation.24 | convolution fusion | flops 3699507200 | bytes 11993088 | tf_op jit(solution)/shard_map/dot_general | solution.py:46
  104.2 0.0 copy-start.1
  104.2 4.1 %all-to-all-start = ((bf16[4,160,2048]{2,1,0:T(8,128)(2,1)}), bf16[4,160,2048]{2,1,0:T(8,128)(2,1)S(1)}, u32[]{:S(2)}, u32[]{:S(2)}) async-start(bf16[4,160,2048]{2,1,0:T(8,128)(2,1)} %bitcast.13), calls=%async_computation | async-start | bytes 5242880 | tf_op jit(solution)/shard_map/all_to_all | solution.py:29
  108.3 0.0 copy-done.1
  108.3 0.3 copy.13
  108.6 11.9 %fusion.13 = (bf16[640,1408]{1,0:T(8,128)(2,1)}, bf16[640,1408]{1,0:T(8,128)(2,1)}) fusion(bf16[640,1408]{1,0:T(8,128)(2,1)} %param.9, bf16[640,1408]{1,0:T(8,128)(2,1)} %param.10, bf16[640,2048]{1,0:T(8,128)(2,1)} %bitcast.12, bf16[1408,2048]{0,1:T(8,128)(2,1)} %all-gather.2.cloned.1.call-done), kind=kOutput, calls=%fused_computation.22 | convolution fusion | flops 3704504320 | bytes 15597568 | tf_op jit(solution)/shard_map/dot_general | solution.py:50
  120.5 19.3 %all-to-all-done = bf16[4,160,2048]{2,1,0:T(8,128)(2,1)S(1)} async-done(((bf16[4,160,2048]{2,1,0:T(8,128)(2,1)}), bf16[4,160,2048]{2,1,0:T(8,128)(2,1)S(1)}, u32[]{:S(2)}, u32[]{:S(2)}) %all-to-all-start) | async-done | bytes 2621472 | tf_op jit(solution)/shard_map/all_to_all | solution.py:29
  139.8 1.5 reduce_sum.12
  141.3 109.3 %reduce-scatter.4.cloned.1.call-done = f32[32,1408]{1,0:T(8,128)} async-done(((f32[2048,1408]{1,0:T(8,128)}), f32[32,1408]{1,0:T(8,128)}) %reduce-scatter.4.cloned.1.call-update) | async-done | bytes 180240
  250.5 1.2 copy.16
  251.7 0.1 bitcast_add_fusion
  251.8 0.9 copy.14
Async XLA Ops:
  7.2 87.8 %all-gather.2.cloned.1.call-start = ((), (), s32[]{:S(2)}) async-start(), calls=%async_computation.3 | async-start | bytes 5857280 | tf_op jit(solution)/shard_map/all_gather | solution.py:44
  7.9 38.8 %copy-start.3 = (bf16[640,1408]{1,0:T(8,128)(2,1)S(1)}, bf16[640,1408]{1,0:T(8,128)(2,1)}, u32[]{:S(2)}) copy-start(bf16[640,1408]{1,0:T(8,128)(2,1)} %param.9) | copy-start | bytes 5406724
  7.9 242.6 %reduce-scatter.4.cloned.1.call-start = ((), (), s32[]{:S(2)}) async-start(), calls=%async_computation.4 | async-start | bytes 11714560
  8.0 38.7 %copy-start.4 = (bf16[640,1408]{1,0:T(8,128)(2,1)S(1)}, bf16[640,1408]{1,0:T(8,128)(2,1)}, u32[]{:S(2)}) copy-start(bf16[640,1408]{1,0:T(8,128)(2,1)} %param.10) | copy-start | bytes 5406724
  45.1 1.5 copy-start
  66.6 28.4 %copy-start.2 = (bf16[640,1408]{1,0:T(8,128)(2,1)S(1)}, bf16[640,1408]{1,0:T(8,128)(2,1)}, u32[]{:S(2)}) copy-start(bf16[640,1408]{1,0:T(8,128)(2,1)} %param.8) | copy-start | bytes 5406724
  104.2 4.1 %copy-start.1 = (f32[1408,32]{0,1:T(8,128)S(1)}, f32[1408,32]{0,1:T(8,128)}, u32[]{:S(2)}) copy-start(f32[1408,32]{0,1:T(8,128)} %param.13) | copy-start | bytes 540676
  104.2 35.6 %all-to-all-start = ((bf16[4,160,2048]{2,1,0:T(8,128)(2,1)}), bf16[4,160,2048]{2,1,0:T(8,128)(2,1)S(1)}, u32[]{:S(2)}, u32[]{:S(2)}) async-start(bf16[4,160,2048]{2,1,0:T(8,128)(2,1)} %bitcast.13), calls=%async_computation | async-start | bytes 5242880 | tf_op jit(solution)/shard_map/all_to_all | solution.py:29
Sparse Core Ops, SparseCore 0:
  10.7 84.2 all-gather.1
  99.3 151.1 reduce-scatter.3
where the time goes:
time: 264 us; the launch traced here: 260 us
  waiting for transfers between devices  158 us (60%)
  blocking collectives  35.6 us (13%)
  matrix products  29 us (11%)
  local copies, waits for them, and re-layouts  17.5 us (7%)
  between operations  14.1 us (5%)
  starting transfers between devices  4.18 us (2%)
    unnamed x3, waiting for transfers between devices  110 us
    all_to_all x1, blocking collectives, copy_for_each(): lax.all_to_all(jnp.broadcast_to(x[None], (size, *x.shape)), axis, 0, 0, t...  35.6 us
    all_gather x1, waiting for transfers between devices, on_device(): whole = lax.all_gather(down_weight, 'fs', axis=1, tiled=True)  28.3 us
    all_to_all x1, waiting for transfers between devices, sent_and_summed(): lax.all_to_all(tiles, axis, split_axis=0, concat_axis=0, tiled=True)  19.3 us
    unnamed x14, local copies, waits for them, and re-layouts  16 us
    dot_general x1, matrix products, on_device(): lax.dot_general(cot_rows, whole, (((1,), (1,)), ((), ())), preferred_elem...  11.9 us
    dot_general x1, matrix products, on_device(): jnp.dot(later_hidden, whole, preferred_element_type=jnp.float32)  9.17 us
    dot_general x1, matrix products, on_device(): lax.dot_general(cot_rows, early_hidden, (((0,), (0,)), ((), ())), preferr...  7.87 us
  transfers between devices with their start and end apart: 3, of which 3 were waited for; matrix products, arithmetic and copies ran while one was open for 17% of the time, Pallas kernels for 0%

commit v1 on v0

v1 whole, which is shorter than its diff:
```python
import functools

import jax
import jax.numpy as jnp
from jax import lax
from jax.experimental import pallas as pl
from jax.experimental.pallas import tpu as pltpu
from jax.sharding import PartitionSpec as P

MESH = pl.DeviceIdType.MESH
F32, BF16 = jnp.float32, jnp.bfloat16
NX, NY, NZ, NC = 4, 4, 8, 2
ROWS = 32
WIDE = NY * NC * ROWS
TILE = 16


def sigmoid(v):
    return 0.5 * jnp.tanh(0.5 * v) + 0.5


def kernel(
    lg_h, lu_h, eg_h, eu_h, cot_h, wt_h,
    mixed_o, gg_o, ug_o, gsum_o,
    lg, lu, eg, eu, eh, cot, wt, gbuf, precv, zrecv, yrecv, pbuf, pre, full, mixed, hc, gsum,
    load_sem, out_sem,
    cd_s, cd_r, cf_s, cf_r,
    wz_s, wz_r, wy_s, wy_r, wf_s, wf_r, wd_s, wd_r,
    gp_s, gp_r, gz_s, gz_r, gy_s, gy_r,
    mp_s, mp_r, mf_s, mf_r,
):
    f, x = lax.axis_index("fs"), lax.axis_index("tp")
    c, y, z = lax.rem(f, NC), lax.rem(f // NC, NY), f // (NC * NY)
    xrows = cot_h.shape[0]
    half = xrows // 2
    hrow = ROWS // 2
    tokens = NX * xrows

    def dx(k):
        return lax.rem(x + (k + NX), NX)

    def dy(k):
        return lax.rem(y + (k + NY), NY)

    def dz(k):
        return lax.rem(z + (k + NZ), NZ)

    def at_x(k):
        return (f, dx(k))

    def at_y(k):
        return ((z * NY + dy(k)) * NC + c, x)

    def at_z(k):
        return ((dz(k) * NY + y) * NC + c, x)

    partner = ((z * NY + y) * NC + (1 - c), x)

    sends, outs = [], []

    def send(src, dst, ssem, rsem, to):
        copy = pltpu.make_async_remote_copy(
            src_ref=src, dst_ref=dst, send_sem=ssem, recv_sem=rsem, device_id=to, device_id_type=MESH
        )
        copy.start()
        sends.append(copy)

    def arrived(dst, ssem, rsem):
        pltpu.make_async_remote_copy(
            src_ref=dst, dst_ref=dst, send_sem=ssem, recv_sem=rsem, device_id=partner, device_id_type=MESH
        ).wait_recv()

    loads = [
        pltpu.make_async_copy(src, dst, load_sem.at[i])
        for i, (src, dst) in enumerate(
            [
                (eg_h, eg),
                (eu_h, eu),
                (cot_h, cot.at[pl.ds(pl.multiple_of(x * xrows, TILE), xrows)]),
                (wt_h, wt.at[z * NY + y, c]),
                (lg_h, lg),
                (lu_h, lu),
            ]
        )
    ]
    for copy in loads:
        copy.start()

    barrier = pltpu.get_barrier_semaphore()
    peers = [at_x(1), at_x(-1), at_y(1), at_y(-1), at_y(2), at_z(1), at_z(-1), partner]
    for peer in peers:
        pl.semaphore_signal(barrier, inc=1, device_id=peer, device_id_type=MESH)
    pl.semaphore_wait(barrier, len(peers))

    SIDES = ((0, 1), (1, -1))
    ZSTEPS = (4, 3, -3, 2, -2, 1, -1, 0)
    WSTEPS = (0, -1, 1, -2, 2, -3, 3, 4)

    def columns(step):
        return pl.ds(pl.multiple_of(dz(step) * WIDE, WIDE), WIDE)

    def cot_rows(step, start=0, size=xrows):
        return pl.ds(pl.multiple_of(dx(step) * xrows + start, TILE), size)

    def cot_direct(k):
        cols = columns(ZSTEPS[k])
        for d, s in SIDES:
            send(cot_h.at[:, cols], cot.at[cot_rows(0), cols], cd_s.at[d, k], cd_r.at[d, k], at_x(s))

    def cot_forward(k):
        cols = columns(ZSTEPS[k])
        for d, s in SIDES:
            block = cot.at[cot_rows(-s), cols]
            arrived(block, cd_s.at[d, k], cd_r.at[d, k])
            part = cot.at[cot_rows(-s, d * half, half), cols]
            send(part, part, cf_s.at[d, k], cf_r.at[d, k], at_x(s))
        if k + 2 < NZ:
            cot_direct(k + 2)

    def cot_done(k):
        cols = columns(ZSTEPS[k])
        for d, s in SIDES:
            part = cot.at[cot_rows(2, d * half, half), cols]
            arrived(part, cf_s.at[d, k], cf_r.at[d, k])

    def w_block(zs, ys):
        return wt.at[dz(zs) * NY + dy(ys), c]

    def w_along_z(s):
        for d, step in SIDES:
            block = w_block(-step * (s - 1), 0)
            if s == 4:
                block = block.at[pl.ds(d * hrow, hrow)]
            send(block, block, wz_s.at[d, s - 1], wz_r.at[d, s - 1], at_z(step))

    def w_along_y(j):
        block = w_block(WSTEPS[j], 0)
        for d, step in SIDES:
            send(block, block, wy_s.at[d, j], wy_r.at[d, j], at_y(step))

    def w_z(s):
        for d, step in SIDES:
            block = w_block(-step * s, 0)
            if s == 4:
                block = block.at[pl.ds(d * hrow, hrow)]
            arrived(block, wz_s.at[d, s - 1], wz_r.at[d, s - 1])
        if s < 4:
            w_along_z(s + 1)
            w_along_y(2 * s - 1)
            w_along_y(2 * s)
        else:
            w_along_y(7)

    def w_y(j):
        for d, step in SIDES:
            block = w_block(WSTEPS[j], -step)
            arrived(block, wy_s.at[d, j], wy_r.at[d, j])
            part = block.at[pl.ds(d * hrow, hrow)]
            send(part, part, wf_s.at[d, j], wf_r.at[d, j], at_y(step))

    def w_core(j):
        for d, step in SIDES:
            part = w_block(WSTEPS[j], 2).at[pl.ds(d * hrow, hrow)]
            arrived(part, wf_s.at[d, j], wf_r.at[d, j])
        rows = wt.at[pl.ds(dz(WSTEPS[j]) * NY, NY), c]
        send(rows, rows, wd_s.at[j], wd_r.at[j], partner)

    def w_done(j):
        rows = wt.at[pl.ds(dz(WSTEPS[j]) * NY, NY), 1 - c]
        arrived(rows, wd_s.at[j], wd_r.at[j])

    def over_rows(first, size, body):
        def step(i, carry):
            body(pl.ds(pl.multiple_of(first + i * TILE, TILE), TILE))
            return carry

        lax.fori_loop(0, size // TILE, step, 0)

    def early(first, size):
        def body(rows):
            gate = eg[rows, :].astype(F32)
            eh[rows, :] = (gate * sigmoid(gate) * eu[rows, :].astype(F32)).astype(BF16)

        over_rows(first, size, body)

    def later(first, size):
        def body(rows):
            gate = lg[rows, :].astype(F32)
            lg[rows, :] = (gate * sigmoid(gate) * lu[rows, :].astype(F32)).astype(BF16)

        over_rows(first, size, body)

    def grad(k):
        cot_done(k)
        part = lax.dot_general(
            cot[:, columns(ZSTEPS[k])], eh[...], (((0,), (0,)), ((), ())), preferred_element_type=F32
        )
        gbuf[k] = part.astype(BF16).reshape(NY, NC, ROWS, part.shape[1])
        send(gbuf.at[k, :, 1 - c], precv.at[k], gp_s.at[k], gp_r.at[k], partner)

    def pair_done(k):
        arrived(precv.at[k], gp_s.at[k], gp_r.at[k])

    def add_up(k, h, more):
        def step(i, carry):
            r, rows = i // 2, pl.ds(pl.multiple_of(lax.rem(i, 2) * TILE, TILE), TILE)
            total = gbuf[k, 2 * h + r, c, rows].astype(F32)
            total += precv[k, 2 * h + r, rows].astype(F32)
            for d, i_at in more:
                total += zrecv[d, i_at, r, rows].astype(F32)
            gbuf[k, 2 * h + r, c, rows] = total.astype(BF16)
            return carry

        lax.fori_loop(0, 4, step, 0)

    CHAIN = (
        ((0, 0), (1, 1), (1, 0), (3, 1), (3, 0), (5, 1), (5, 0)),
        ((0, 1), (2, 0), (2, 1), (4, 0), (4, 1), (6, 0), (6, 1)),
    )

    def chain_arrived(d, i):
        arrived(zrecv.at[d, i], gz_s.at[d, i], gz_r.at[d, i])

    def chain(d, i):
        k, h = CHAIN[d][i]
        if i >= 2:
            chain_arrived(d, i - 2)
        add_up(k, h, [(d, i - 2)] if i >= 2 else [])
        step = SIDES[d][1]
        send(gbuf.at[k, pl.ds(2 * h, 2), c], zrecv.at[d, i], gz_s.at[d, i], gz_r.at[d, i], at_z(step))

    def own_sum():
        for d in (0, 1):
            for i in (5, 6):
                chain_arrived(d, i)
        for h in (0, 1):
            add_up(7, h, [(0, 6 - h), (1, 5 + h)])
        for i, step in enumerate((1, -1, 2)):
            send(gbuf.at[7, dy(step), c], yrecv.at[i], gy_s.at[i], gy_r.at[i], at_y(step))

    def grad_end():
        for i in range(3):
            arrived(yrecv.at[i], gy_s.at[i], gy_r.at[i])
        total = gbuf[7, y, c].astype(F32)
        for i in range(3):
            total += yrecv[i].astype(F32)
        gsum[...] = total
        copy = pltpu.make_async_copy(gsum, gsum_o, out_sem.at[0])
        copy.start()
        outs.append(copy)

    def partial(j):
        w_done(j)
        rows = wt[pl.ds(dz(WSTEPS[j]) * NY, NY)].reshape(WIDE, wt.shape[3])
        part = lax.dot_general(lg[...], rows, (((1,), (1,)), ((), ())), preferred_element_type=F32)
        pbuf[j] = part.astype(BF16).reshape(NX, xrows, WIDE)
        for d, s in SIDES:
            send(pbuf.at[j, dx(2), pl.ds(d * half, half)], pre.at[d, j], mp_s.at[d, j], mp_r.at[d, j], at_x(s))

    def partial_on(j):
        for d, s in SIDES:
            arrived(pre.at[d, j], mp_s.at[d, j], mp_r.at[d, j])
            rows = pl.ds(d * half, half)
            pbuf[j, dx(s), rows] = (pbuf[j, dx(s), rows].astype(F32) + pre[d, j].astype(F32)).astype(BF16)
            send(pbuf.at[j, dx(s)], full.at[d, j], mf_s.at[d, j], mf_r.at[d, j], at_x(s))

    def partial_end(j):
        total = pbuf[j, x].astype(F32)
        for d, s in SIDES:
            arrived(full.at[d, j], mf_s.at[d, j], mf_r.at[d, j])
            total += full[d, j].astype(F32)
        cols = columns(WSTEPS[j])
        mixed[:, cols] = total.astype(BF16)
        copy = pltpu.make_async_copy(mixed.at[:, cols], mixed_o.at[:, cols], out_sem.at[1 + j])
        copy.start()
        outs.append(copy)

    def hidden(m):
        rows = pl.ds(m * xrows, xrows)
        hc[...] = jnp.dot(
            cot[rows, :], wt[...].reshape(NZ * WIDE, wt.shape[3]), preferred_element_type=F32
        )

    def pointwise(m):
        def body(rows):
            sub = pl.ds(rows.start - m * xrows, TILE)
            gate, up, cotan = eg[rows, :].astype(F32), eu[rows, :].astype(F32), hc[sub, :]
            s = sigmoid(gate)
            scaled = cotan * s
            eg[rows, :] = (scaled * up * (1.0 + gate * (1.0 - s))).astype(BF16)
            eu[rows, :] = (scaled * gate).astype(BF16)

        over_rows(m * xrows, xrows, body)
        rows = pl.ds(m * xrows, xrows)
        for i, (src, dst) in enumerate(((eg, gg_o), (eu, ug_o))):
            copy = pltpu.make_async_copy(src.at[rows], dst.at[rows], out_sem.at[9 + 2 * m + i])
            copy.start()
            outs.append(copy)

    tasks = []

    def at(time, run, *args):
        tasks.append((time, len(tasks), run, args))

    def begin():
        cot_direct(0)
        loads[3].wait()
        w_along_z(1)
        w_along_y(0)
        cot_direct(1)
        loads[0].wait()
        loads[1].wait()

    def later_loads():
        loads[4].wait()
        loads[5].wait()

    at(0, begin)
    quarter = tokens // 4
    for i in range(4):
        at(1.2 + 0.75 * i, early, i * quarter, quarter)
    at(3.9, loads[2].wait)
    at(6.0, later_loads)
    for i, t in enumerate((7.5, 8.2, 10.4, 13.0)):
        at(t, later, i * quarter, quarter)
    for k in range(NZ):
        at(3.8 + 2.64 * k, cot_forward, k)
        at(6.5 + 2.64 * k, grad, k)
        at(8.9 + 2.64 * k, pair_done, k)
    for s in range(1, 5):
        at(4.1 * s, w_z, s)
    for j in range(NZ):
        at(4.2 + 2.9 * j, w_y, j)
        at(7.2 + 2.9 * j, w_core, j)
    for d, times in enumerate(
        ((9.0, 11.7, 15.0, 18.9, 22.6, 26.5, 30.4), (9.0, 14.3, 15.1, 19.7, 22.7, 26.6, 30.5))
    ):
        for i, t in enumerate(times):
            at(t, chain, d, i)
    at(38.0, own_sum)
    at(43.5, grad_end)
    for j in range(NZ):
        at(17.0 + 2.6 * j, partial, j)
        at(22.0 + 2.9 * j, partial_on, j)
        at(27.0 + 2.9 * j, partial_end, j)
    for m in range(NX):
        at(35.8 + 1.8 * m, hidden, m)
        at(36.7 + 1.8 * m, pointwise, m)

    for _, _, run, args in sorted(tasks, key=lambda task: task[:2]):
        run(*args)
    for copy in sends:
        copy.wait_send()
    for copy in outs:
        copy.wait()


def on_device(lg, lu, eg, eu, cot, weight, running):
    tokens, block = lg.shape
    xrows, width = cot.shape
    dma, vmem = pltpu.SemaphoreType.DMA, pltpu.VMEM
    shape = jax.ShapeDtypeStruct
    pair = [dma((2, NZ))] * 2
    mixed, gate_grad, up_grad, summed = pl.pallas_call(
        kernel,
        out_shape=(
            shape((xrows, width), BF16),
            shape((tokens, block), BF16),
            shape((tokens, block), BF16),
            shape((ROWS, block), F32),
        ),
        in_specs=[pl.BlockSpec(memory_space=pl.ANY)] * 6,
        out_specs=[pl.BlockSpec(memory_space=pl.ANY)] * 4,
        scratch_shapes=[
            *[vmem((tokens, block), BF16)] * 5,
            vmem((tokens, width), BF16),
            vmem((NZ * NY, NC, ROWS, block), BF16),
            vmem((NZ, NY, NC, ROWS, block), BF16),
            vmem((NZ, NY, ROWS, block), BF16),
            vmem((2, 7, 2, ROWS, block), BF16),
            vmem((3, ROWS, block), BF16),
            vmem((NZ, NX, xrows, WIDE), BF16),
            vmem((2, NZ, xrows // 2, WIDE), BF16),
            vmem((2, NZ, xrows, WIDE), BF16),
            vmem((xrows, width), BF16),
            vmem((xrows, block), F32),
            vmem((ROWS, block), F32),
            dma((6,)),
            dma((17,)),
            *pair,
            *pair,
            *[dma((2, 4))] * 2,
            *pair,
            *pair,
            *[dma((NZ,))] * 2,
            *[dma((NZ,))] * 2,
            *[dma((2, 7))] * 2,
            *[dma((3,))] * 2,
            *pair,
            *pair,
        ],
        compiler_params=pltpu.CompilerParams(
            collective_id=0, has_side_effects=True, vmem_limit_bytes=60 * 1024 * 1024
        ),
        name="layer",
    )(lg, lu, eg, eu, cot, weight.T)
    return (mixed, gate_grad, up_grad, (running.T + summed).T)


def solution(mesh):
    tokens, hidden = P("fs", "tp"), P("tp", "fs")
    rows = P(("fs", "tp"), None)
    return jax.shard_map(
        on_device,
        mesh=mesh,
        in_specs=(tokens, tokens, tokens, tokens, rows, hidden, hidden),
        out_specs=(rows, tokens, tokens, hidden),
        check_vma=False,
    )
```

time: 264 us -> 82.3 us (0.31); the launches traced: 260 us -> 82.1 us
  waiting for transfers between devices: 158 us -> 0 us
  Pallas kernels: 0 us -> 74.4 us
  blocking collectives: 35.6 us -> 0 us
  matrix products: 29 us -> 0 us
  between operations: 14.1 us -> 0.67 us
  local copies, waits for them, and re-layouts: 17.5 us -> 5.35 us
  starting transfers between devices: 4.18 us -> 0 us
    unnamed x3 -> x0, waiting for transfers between devices: 110 us -> none
    pallas_call x0 -> x1, Pallas kernels: none -> 74.4 us  [on_device(): pl.pallas_call(kernel, out_shape=(shape((xrows, width), BF16), shape((tok...]
    all_to_all x1 -> x0, blocking collectives: 35.6 us -> none  [copy_for_each(): lax.all_to_all(jnp.broadcast_to(x[None], (size, *x.shape)), axis, 0, 0, t...]
    dot_general x3 -> x0, matrix products: 29 us -> none  [the longest x1 11.9 us: on_device(): lax.dot_general(cot_rows, whole, (((1,), (1,)), ((), ())), preferred_elem...]
    all_gather x1 -> x0, waiting for transfers between devices: 28.3 us -> none  [on_device(): whole = lax.all_gather(down_weight, 'fs', axis=1, tiled=True)]
    all_to_all x1 -> x0, waiting for transfers between devices: 19.3 us -> none  [sent_and_summed(): lax.all_to_all(tiles, axis, split_axis=0, concat_axis=0, tiled=True)]
    unnamed x14 -> x9, local copies, waits for them, and re-layouts: 16 us -> 5.35 us
    all_to_all x1 -> x0, starting transfers between devices: 4.1 us -> none  [sent_and_summed(): lax.all_to_all(tiles, axis, split_axis=0, concat_axis=0, tiled=True)]
  transfers between devices with their start and end apart: 3 -> 0, of which waited for: 3 -> 0; matrix products, arithmetic and copies ran while one was open for 17% -> 0% of each run, Pallas kernels for 0% -> 0%
where the time goes in v1:
time: 82.3 us; the launch traced here: 82.1 us
  Pallas kernels  74.4 us (90%)
  local copies, waits for them, and re-layouts  5.35 us (7%)
  other arithmetic  1.74 us (2%)
    pallas_call x1, Pallas kernels, on_device(): pl.pallas_call(kernel, out_shape=(shape((xrows, width), BF16), shape((tok...  74.4 us
    unnamed x9, local copies, waits for them, and re-layouts  5.35 us
    transpose x1, other arithmetic, on_device(): return (mixed, gate_grad, up_grad, (running.T + summed).T)  1.74 us

profile of v1, /device:TPU:1, one launch (start us, length us, event | category | flops | bytes accessed | tf_op | source)
XLA Modules:
  0.0 82.1 jit_solution(17883449340851676925)
XLA Ops:
  0.6 0.0 copy-start.2
  0.6 74.4 %layer.1 = (bf16[160,2048]{1,0:T(8,128)(2,1)}, bf16[640,1408]{1,0:T(8,128)(2,1)}, bf16[640,1408]{1,0:T(8,128)(2,1)}, f32[32,1408]{1,0:T(8,128)}) custom-call(bf16[640,1408]{1,0:T(8,128)(2,1)} %lg_h.1, bf16[640,1408]{1,0:T(8,128)(2,1)} %lu_h.1, bf16[640,1408]{1,0:T(8,128)(2,1)} %eg_h.1, bf16[640,1408]{1,0:T(8,128)(2,1)} %eu_h.1, bf16[160,2048]{1,0:T(8,128)(2,1)} %cot_h.1, ...), custom_call_target="tpu_custom_call" | custom-call | tf_op jit(solution)/shard_map/layer/pallas_call | solution.py:364
  75.0 0.0 copy-start.1
  75.0 0.0 copy-done.2
  75.0 1.7 %fusion = f32[1408,32]{0,1:T(8,128)} fusion(f32[32,1408]{1,0:T(8,128)} %get-tuple-element.11, f32[1408,32]{0,1:T(8,128)S(1)} %copy-done.2), kind=kLoop, calls=%fused_computation.1 | loop fusion | flops 45056 | bytes 540672 | tf_op jit(solution)/shard_map/transpose | solution.py:407
  76.8 2.0 %copy.14 = bf16[160,2048]{1,0:T(8,128)(2,1)} copy(bf16[160,2048]{1,0:T(8,128)(2,1)} %get-tuple-element.16) | data formatting | bytes 1310720
  78.7 0.0 copy-done.1
  78.8 0.0 copy-start
  78.8 1.2 %copy.15 = bf16[640,1408]{1,0:T(8,128)(2,1)} copy(bf16[640,1408]{1,0:T(8,128)(2,1)S(1)} %copy-done.1) | data formatting | bytes 3604480
  80.0 0.9 %copy-done = bf16[640,1408]{1,0:T(8,128)(2,1)S(1)} copy-done((bf16[640,1408]{1,0:T(8,128)(2,1)S(1)}, bf16[640,1408]{1,0:T(8,128)(2,1)}, u32[]{:S(2)}) %copy-start) | copy-done | bytes 1802264
  80.9 1.2 %copy.16 = bf16[640,1408]{1,0:T(8,128)(2,1)} copy(bf16[640,1408]{1,0:T(8,128)(2,1)S(1)} %copy-done) | data formatting | bytes 3604480
Async XLA Ops:
  0.6 74.4 %copy-start.2 = (f32[1408,32]{0,1:T(8,128)S(1)}, f32[1408,32]{0,1:T(8,128)}, u32[]{:S(2)}) copy-start(f32[1408,32]{0,1:T(8,128)} %param.13) | copy-start | bytes 540676
  75.0 3.7 %copy-start.1 = (bf16[640,1408]{1,0:T(8,128)(2,1)S(1)}, bf16[640,1408]{1,0:T(8,128)(2,1)}, u32[]{:S(2)}) copy-start(bf16[640,1408]{1,0:T(8,128)(2,1)} %get-tuple-element.17) | copy-start | bytes 5406724
  78.8 2.1 %copy-start = (bf16[640,1408]{1,0:T(8,128)(2,1)S(1)}, bf16[640,1408]{1,0:T(8,128)(2,1)}, u32[]{:S(2)}) copy-start(bf16[640,1408]{1,0:T(8,128)(2,1)} %get-tuple-element.18) | copy-start | bytes 5406724

commit v2 on v1

v2 whole, which is shorter than its diff:
```python
import functools

import jax
import jax.numpy as jnp
from jax import lax
from jax.experimental import pallas as pl
from jax.experimental.pallas import tpu as pltpu
from jax.sharding import PartitionSpec as P

MESH = pl.DeviceIdType.MESH
F32, BF16 = jnp.float32, jnp.bfloat16
NX, NY, NZ, NC = 4, 4, 8, 2
ROWS = 32
WIDE = NY * NC * ROWS
TILE = 16


ORDER = (
    "B", "e0", "e1", "e2", "e3", "c", "L", "l0", "l1", "l2", "l3", "z1", "y0", "f0", "f1", "g0", "z2", "y1", "f2",
    "y2", "g1", "d0", "u0", "u1", "v0", "v1", "k0", "f3", "g2", "d1", "u2", "u3", "z3", "y3", "f4", "p0", "u4", "d2",
    "v2", "v3", "y4", "k1", "g3", "f5", "k2", "u5", "v4", "v5", "p1", "d3", "y5", "g4", "u6", "f6", "p2", "u7", "q0",
    "y6", "k3", "g5", "d4", "v6", "v7", "z4", "k4", "f7", "k5", "p3", "u8", "v8", "d5", "q1", "g6", "u9", "v9", "q2",
    "k6", "p4", "y7", "p5", "u10", "d6", "v10", "g7", "u11", "v11", "q3", "p6", "k7", "r0", "u12", "r1", "v12", "d7",
    "r2", "q4", "u13", "p7", "v13", "q5", "h0", "r3", "w0", "h1", "o2", "q6", "w1", "h2", "o0", "o1", "q7", "r4",
    "w2", "h3", "r5", "w3", "r6", "r7", "G",
)


def sigmoid(v):
    return 0.5 * jnp.tanh(0.5 * v) + 0.5


def kernel(
    lg_h, lu_h, eg_h, eu_h, cot_h, wt_h, running_h,
    mixed, eg, eu, gsum,
    lg, lu, eh, cot, wt, gbuf, precv, zrecv, yrecv, pbuf, pre, full, hc,
    load_sem, sent,
    cd_r, cf_r, wz_r, wy_r, wf_r, wd_r, gp_r, gz_r, gy_r, mp_r, mf_r,
):
    f, x = lax.axis_index("fs"), lax.axis_index("tp")
    c, y, z = lax.rem(f, NC), lax.rem(f // NC, NY), f // (NC * NY)
    xrows = cot_h.shape[0]
    half = xrows // 2
    hrow = ROWS // 2
    tokens = NX * xrows

    def dx(k):
        return lax.rem(x + (k + NX), NX)

    def dy(k):
        return lax.rem(y + (k + NY), NY)

    def dz(k):
        return lax.rem(z + (k + NZ), NZ)

    def at_x(k):
        return (f, dx(k))

    def at_y(k):
        return ((z * NY + dy(k)) * NC + c, x)

    def at_z(k):
        return ((dz(k) * NY + y) * NC + c, x)

    partner = ((z * NY + y) * NC + (1 - c), x)

    def send(src, dst, kind, rsem, to):
        pltpu.make_async_remote_copy(
            src_ref=src, dst_ref=dst, send_sem=sent.at[kind], recv_sem=rsem, device_id=to, device_id_type=MESH
        ).start()

    def arrived(dst, rsem):
        pltpu.make_async_remote_copy(
            src_ref=dst, dst_ref=dst, send_sem=sent.at[0], recv_sem=rsem, device_id=partner, device_id_type=MESH
        ).wait_recv()

    def all_sent(kind, like):
        pltpu.make_async_remote_copy(
            src_ref=like, dst_ref=like, send_sem=sent.at[kind], recv_sem=cd_r.at[0, 0], device_id=partner, device_id_type=MESH
        ).wait_send()

    loads = [
        pltpu.make_async_copy(src, dst, load_sem.at[i])
        for i, (src, dst) in enumerate(
            [
                (eg_h, eg),
                (eu_h, eu),
                (cot_h, cot.at[pl.ds(pl.multiple_of(x * xrows, TILE), xrows)]),
                (wt_h, wt.at[z * NY + y, c]),
                (lg_h, lg),
                (lu_h, lu),
                (running_h, gsum),
            ]
        )
    ]
    for copy in loads:
        copy.start()

    barrier = pltpu.get_barrier_semaphore()
    peers = [at_x(1), at_x(-1), at_y(1), at_y(-1), at_y(2), at_z(1), at_z(-1), partner]
    for peer in peers:
        pl.semaphore_signal(barrier, inc=1, device_id=peer, device_id_type=MESH)
    pl.semaphore_wait(barrier, len(peers))

    SIDES = ((0, 1), (1, -1))
    ZSTEPS = (4, 3, -3, 2, -2, 1, -1, 0)
    WSTEPS = (0, -1, 1, -2, 2, -3, 3, 4)

    def columns(step):
        return pl.ds(pl.multiple_of(dz(step) * WIDE, WIDE), WIDE)

    def cot_rows(step, start=0, size=xrows):
        return pl.ds(pl.multiple_of(dx(step) * xrows + start, TILE), size)

    def cot_direct(k):
        cols = columns(ZSTEPS[k])
        for d, s in SIDES:
            send(cot_h.at[:, cols], cot.at[cot_rows(0), cols], 0, cd_r.at[d, k], at_x(s))

    def cot_forward(k):
        cols = columns(ZSTEPS[k])
        for d, s in SIDES:
            block = cot.at[cot_rows(-s), cols]
            arrived(block, cd_r.at[d, k])
            part = cot.at[cot_rows(-s, d * half, half), cols]
            send(part, part, 1, cf_r.at[d, k], at_x(s))
        if k + 2 < NZ:
            cot_direct(k + 2)

    def cot_done(k):
        cols = columns(ZSTEPS[k])
        for d, s in SIDES:
            part = cot.at[cot_rows(2, d * half, half), cols]
            arrived(part, cf_r.at[d, k])

    def w_block(zs, ys):
        return wt.at[dz(zs) * NY + dy(ys), c]

    def w_along_z(s):
        for d, step in SIDES:
            block = w_block(-step * (s - 1), 0)
            if s == 4:
                block = block.at[pl.ds(d * hrow, hrow)]
            send(block, block, 2, wz_r.at[d, s - 1], at_z(step))

    def w_along_y(j):
        block = w_block(WSTEPS[j], 0)
        for d, step in SIDES:
            send(block, block, 3, wy_r.at[d, j], at_y(step))

    def w_z(s):
        for d, step in SIDES:
            block = w_block(-step * s, 0)
            if s == 4:
                block = block.at[pl.ds(d * hrow, hrow)]
            arrived(block, wz_r.at[d, s - 1])
        if s < 4:
            w_along_z(s + 1)
            w_along_y(2 * s - 1)
            w_along_y(2 * s)
        else:
            w_along_y(7)

    def w_y(j):
        for d, step in SIDES:
            block = w_block(WSTEPS[j], -step)
            arrived(block, wy_r.at[d, j])
            part = block.at[pl.ds(d * hrow, hrow)]
            send(part, part, 4, wf_r.at[d, j], at_y(step))

    def w_core(j):
        for d, step in SIDES:
            part = w_block(WSTEPS[j], 2).at[pl.ds(d * hrow, hrow)]
            arrived(part, wf_r.at[d, j])
        rows = wt.at[pl.ds(dz(WSTEPS[j]) * NY, NY), c]
        send(rows, rows, 5, wd_r.at[j], partner)

    def w_done(j):
        rows = wt.at[pl.ds(dz(WSTEPS[j]) * NY, NY), 1 - c]
        arrived(rows, wd_r.at[j])

    def over_rows(first, size, body):
        def step(i, carry):
            body(pl.ds(pl.multiple_of(first + i * TILE, TILE), TILE))
            return carry

        lax.fori_loop(0, size // TILE, step, 0)

    def early(first, size):
        def body(rows):
            gate = eg[rows, :].astype(F32)
            eh[rows, :] = (gate * sigmoid(gate) * eu[rows, :].astype(F32)).astype(BF16)

        over_rows(first, size, body)

    def later(first, size):
        def body(rows):
            gate = lg[rows, :].astype(F32)
            lg[rows, :] = (gate * sigmoid(gate) * lu[rows, :].astype(F32)).astype(BF16)

        over_rows(first, size, body)

    def grad(k):
        cot_done(k)
        part = lax.dot_general(
            cot[:, columns(ZSTEPS[k])], eh[...], (((0,), (0,)), ((), ())), preferred_element_type=F32
        )
        gbuf[k] = part.astype(BF16).reshape(NY, NC, ROWS, part.shape[1])
        send(gbuf.at[k, :, 1 - c], precv.at[k], 6, gp_r.at[k], partner)

    def pair_done(k):
        arrived(precv.at[k], gp_r.at[k])

    def add_up(k, r, more):
        total = gbuf[k, dy(r), c].astype(F32) + precv[k, dy(r)].astype(F32)
        for d, i in more:
            total += zrecv[d, i].astype(F32)
        return total

    CHAIN = (
        ((0, -1), (0, 0), *((k, r) for k in (1, 3, 5) for r in (2, 1, -1, 0))),
        ((0, 2), (0, 1), *((k, r) for k in (2, 4, 6) for r in (-1, 2, 1, 0))),
    )

    def chain_before(d, k, r):
        nearer = ((1, 3, 5, 7), (2, 4, 6, 7))[d]
        before = (((0,) + nearer)[nearer.index(k)], r) if k in nearer else None
        if before not in CHAIN[d]:
            return []
        i = CHAIN[d].index(before)
        arrived(zrecv.at[d, i], gz_r.at[d, i])
        return [(d, i)]

    def chain(d, i):
        k, r = CHAIN[d][i]
        gbuf[k, dy(r), c] = add_up(k, r, chain_before(d, k, r)).astype(BF16)
        send(gbuf.at[k, dy(r), c], zrecv.at[d, i], 7, gz_r.at[d, i], at_z(SIDES[d][1]))

    def own_sum(i):
        r = (1, -1, 2)[i]
        gbuf[7, dy(r), c] = add_up(7, r, chain_before(0, 7, r) + chain_before(1, 7, r)).astype(BF16)
        send(gbuf.at[7, dy(r), c], yrecv.at[i], 8, gy_r.at[i], at_y(r))

    def grad_end():
        total = add_up(7, 0, chain_before(0, 7, 0) + chain_before(1, 7, 0))
        for i in range(3):
            arrived(yrecv.at[i], gy_r.at[i])
            total += yrecv[i].astype(F32)
        gsum[...] += total

    def partial(j):
        w_done(j)
        rows = wt[pl.ds(dz(WSTEPS[j]) * NY, NY)].reshape(WIDE, wt.shape[3])
        part = lax.dot_general(lg[...], rows, (((1,), (1,)), ((), ())), preferred_element_type=F32)
        pbuf[j] = part.astype(BF16).reshape(NX, xrows, WIDE)
        for d, s in SIDES:
            send(pbuf.at[j, dx(2), pl.ds(d * half, half)], pre.at[d, j], 9, mp_r.at[d, j], at_x(s))

    def partial_on(j):
        for d, s in SIDES:
            arrived(pre.at[d, j], mp_r.at[d, j])
            rows = pl.ds(d * half, half)
            pbuf[j, dx(s), rows] = (pbuf[j, dx(s), rows].astype(F32) + pre[d, j].astype(F32)).astype(BF16)
            send(pbuf.at[j, dx(s)], full.at[d, j], 10, mf_r.at[d, j], at_x(s))

    def partial_end(j):
        total = pbuf[j, x].astype(F32)
        for d, s in SIDES:
            arrived(full.at[d, j], mf_r.at[d, j])
            total += full[d, j].astype(F32)
        cols = columns(WSTEPS[j])
        mixed[:, cols] = total.astype(BF16)

    def hidden(m):
        rows = pl.ds(m * xrows, xrows)
        hc[...] = jnp.dot(
            cot[rows, :], wt[...].reshape(NZ * WIDE, wt.shape[3]), preferred_element_type=F32
        )

    def pointwise(m):
        def body(rows):
            sub = pl.ds(rows.start - m * xrows, TILE)
            gate, up, cotan = eg[rows, :].astype(F32), eu[rows, :].astype(F32), hc[sub, :]
            s = sigmoid(gate)
            scaled = cotan * s
            eg[rows, :] = (scaled * up * (1.0 + gate * (1.0 - s))).astype(BF16)
            eu[rows, :] = (scaled * gate).astype(BF16)

        over_rows(m * xrows, xrows, body)

    def begin():
        cot_direct(0)
        loads[3].wait()
        w_along_z(1)
        w_along_y(0)
        cot_direct(1)
        loads[0].wait()
        loads[1].wait()

    def later_loads():
        for copy in loads[4:]:
            copy.wait()

    quarter = tokens // 4
    tasks = {
        "B": begin,
        "e": lambda i: early(i * quarter, quarter),
        "c": loads[2].wait,
        "L": later_loads,
        "l": lambda i: later(i * quarter, quarter),
        "f": cot_forward,
        "g": grad,
        "d": pair_done,
        "z": w_z,
        "y": w_y,
        "k": w_core,
        "u": lambda i: chain(0, i),
        "v": lambda i: chain(1, i),
        "o": own_sum,
        "G": grad_end,
        "p": partial,
        "q": partial_on,
        "r": partial_end,
        "h": hidden,
        "w": pointwise,
    }
    for task in ORDER:
        tasks[task[0]](*(int(i) for i in task[1:].split("_") if i))
    for kind, like in enumerate(
        (full, pre, wt.at[pl.ds(0, 7), 0], wt.at[pl.ds(0, 16), 0], wt.at[pl.ds(0, 8), 0], precv, precv,
         wt.at[pl.ds(0, 28), 0], yrecv, pre, full)
    ):
        all_sent(kind, like)


def on_device(lg, lu, eg, eu, cot, weight, running):
    tokens, block = lg.shape
    xrows, width = cot.shape
    dma, vmem = pltpu.SemaphoreType.DMA, pltpu.VMEM
    mixed, gate_grad, up_grad, total = pl.pallas_call(
        kernel,
        out_shape=(
            vmem((xrows, width), BF16),
            vmem((tokens, block), BF16),
            vmem((tokens, block), BF16),
            vmem((ROWS, block), F32),
        ),
        in_specs=[pl.BlockSpec(memory_space=pl.ANY)] * 7,
        out_specs=[pl.BlockSpec(memory_space=vmem)] * 4,
        scratch_shapes=[
            *[vmem((tokens, block), BF16)] * 3,
            vmem((tokens, width), BF16),
            vmem((NZ * NY, NC, ROWS, block), BF16),
            vmem((NZ, NY, NC, ROWS, block), BF16),
            vmem((NZ, NY, ROWS, block), BF16),
            vmem((2, 14, ROWS, block), BF16),
            vmem((3, ROWS, block), BF16),
            vmem((NZ, NX, xrows, WIDE), BF16),
            vmem((2, NZ, xrows // 2, WIDE), BF16),
            vmem((2, NZ, xrows, WIDE), BF16),
            vmem((xrows, block), F32),
            dma((7,)),
            dma((11,)),
            dma((2, NZ)),
            dma((2, NZ)),
            dma((2, 4)),
            dma((2, NZ)),
            dma((2, NZ)),
            dma((NZ,)),
            dma((NZ,)),
            dma((2, 14)),
            dma((3,)),
            dma((2, NZ)),
            dma((2, NZ)),
        ],
        compiler_params=pltpu.CompilerParams(
            collective_id=0, has_side_effects=True, vmem_limit_bytes=52 * 1024 * 1024
        ),
        name="layer",
    )(lg, lu, eg, eu, cot, weight.T, running.T)
    return (mixed, gate_grad, up_grad, total.T)


def solution(mesh):
    tokens, hidden = P("fs", "tp"), P("tp", "fs")
    rows = P(("fs", "tp"), None)
    return jax.shard_map(
        on_device,
        mesh=mesh,
        in_specs=(tokens, tokens, tokens, tokens, rows, hidden, hidden),
        out_specs=(rows, tokens, tokens, hidden),
        check_vma=False,
    )
```

time: 82.3 us -> 61 us (0.74)
  Pallas kernels: 74.4 us -> 56.3 us
  other arithmetic: 1.74 us -> 0 us
  local copies, waits for them, and re-layouts: 5.35 us -> 3.94 us
    pallas_call x1, Pallas kernels: 74.4 us -> 56.3 us  [on_device(): pl.pallas_call(kernel, out_shape=(vmem((xrows, width), BF16), vmem((token...]
    transpose x1 -> x0, other arithmetic: 1.74 us -> none  [on_device(): return (mixed, gate_grad, up_grad, (running.T + summed).T)]
    unnamed x9 -> x4, local copies, waits for them, and re-layouts: 5.35 us -> 3.94 us
where the time goes in v2:
time: 61 us; the launch traced here: 60.9 us
  Pallas kernels  56.3 us (92%)
  local copies, waits for them, and re-layouts  3.94 us (6%)
  between operations  0.64 us (1%)
    pallas_call x1, Pallas kernels, on_device(): pl.pallas_call(kernel, out_shape=(vmem((xrows, width), BF16), vmem((token...  56.3 us
    unnamed x4, local copies, waits for them, and re-layouts  3.94 us

profile of v2, /device:TPU:1, one launch (start us, length us, event | category | flops | bytes accessed | tf_op | source)
XLA Modules:
  0.0 60.9 jit_solution(9240636279840717809)
XLA Ops:
  0.6 56.3 %layer.1 = (bf16[160,2048]{1,0:T(8,128)(2,1)S(1)}, bf16[640,1408]{1,0:T(8,128)(2,1)S(1)}, bf16[640,1408]{1,0:T(8,128)(2,1)S(1)}, f32[32,1408]{1,0:T(8,128)S(1)}) custom-call(bf16[640,1408]{1,0:T(8,128)(2,1)} %lg_h.1, bf16[640,1408]{1,0:T(8,128)(2,1)} %lu_h.1, bf16[640,1408]{1,0:T(8,128)(2,1)} %eg_h.1, bf16[640,1408]{1,0:T(8,128)(2,1)} %eu_h.1, ...), custom_call_target="tpu_custom_call" | custom-call | tf_op jit(solution)/shard_map/layer/pallas_call | solution.py:340
  57.0 0.8 %copy.15 = bf16[160,2048]{1,0:T(8,128)(2,1)} copy(bf16[160,2048]{1,0:T(8,128)(2,1)S(1)} %get-tuple-element.12) | data formatting | bytes 1310720
  57.8 0.7 %copy.18 = f32[1408,32]{0,1:T(8,128)} copy(f32[1408,32]{0,1:T(8,128)S(1)} %bitcast.3) | data formatting | bytes 360448
  58.5 1.2 %copy.16 = bf16[640,1408]{1,0:T(8,128)(2,1)} copy(bf16[640,1408]{1,0:T(8,128)(2,1)S(1)} %get-tuple-element.13) | data formatting | bytes 3604480
  59.7 1.2 %copy.17 = bf16[640,1408]{1,0:T(8,128)(2,1)} copy(bf16[640,1408]{1,0:T(8,128)(2,1)S(1)} %get-tuple-element.14) | data formatting | bytes 3604480

commit v3 on v2

--- a/solution.py
+++ b/solution.py
@@ -13,16 +13,21 @@
 ROWS = 32
 WIDE = NY * NC * ROWS
 TILE = 16
+AHEAD = ((2,), (3,), (4, 5), (6,), (7,), (), (), ())
+CUT = 1024
+KCUT = 768
+PARTS = 2
 
 
 ORDER = (
-    "B", "e0", "e1", "e2", "e3", "c", "L", "l0", "l1", "l2", "l3", "z1", "y0", "f0", "f1", "g0", "z2", "y1", "f2",
-    "y2", "g1", "d0", "u0", "u1", "v0", "v1", "k0", "f3", "g2", "d1", "u2", "u3", "z3", "y3", "f4", "p0", "u4", "d2",
-    "v2", "v3", "y4", "k1", "g3", "f5", "k2", "u5", "v4", "v5", "p1", "d3", "y5", "g4", "u6", "f6", "p2", "u7", "q0",
-    "y6", "k3", "g5", "d4", "v6", "v7", "z4", "k4", "f7", "k5", "p3", "u8", "v8", "d5", "q1", "g6", "u9", "v9", "q2",
-    "k6", "p4", "y7", "p5", "u10", "d6", "v10", "g7", "u11", "v11", "q3", "p6", "k7", "r0", "u12", "r1", "v12", "d7",
-    "r2", "q4", "u13", "p7", "v13", "q5", "h0", "r3", "w0", "h1", "o2", "q6", "w1", "h2", "o0", "o1", "q7", "r4",
-    "w2", "h3", "r5", "w3", "r6", "r7", "G",
+    "B", "e0", "e1", "e2", "e3", "c", "L", "l0", "l1", "l2", "z1_0", "l3", "z1_1", "y0", "f0", "f1", "z2_0", "g0",
+    "z2_1", "y1", "f2", "z3_0", "g1", "d0", "u0", "u1", "v0", "v1", "y2", "k0", "z3_1", "f3", "z4_0", "g2", "d1",
+    "u2", "u3", "y3", "f4", "p0", "u4", "y4", "d2", "v2", "v3", "k1", "f5", "k2", "u5", "v4", "v5", "g3", "z4_1",
+    "p1", "f6", "y5", "p2", "g4", "d3", "u6", "y6", "u7", "f7", "k3", "q0", "d4", "v6", "u8", "v7", "k4", "g5", "v8",
+    "q1", "p3", "u9", "y7", "p4", "v9", "k5", "g6", "d5", "u10", "q2", "k6", "g7", "p5", "u11", "k7", "r0", "d6",
+    "v10", "p6", "r1", "d7", "u12", "p7", "v11", "v12", "q3", "h0_0", "u13", "q4", "h0_1", "v13", "w0", "r2", "h1_0",
+    "q5", "h1_1", "o0", "q6", "w1", "h2_0", "q7", "h2_1", "o1", "w2", "r3", "h3_0", "o2", "h3_1", "w3", "r4", "r5",
+    "r6", "G", "r7",
 )
 
 
@@ -76,8 +81,13 @@
 
     def all_sent(kind, like):
         pltpu.make_async_remote_copy(
-            src_ref=like, dst_ref=like, send_sem=sent.at[kind], recv_sem=cd_r.at[0, 0], device_id=partner, device_id_type=MESH
+            src_ref=like, dst_ref=like, send_sem=sent.at[kind], recv_sem=cd_r.at[0], device_id=partner, device_id_type=MESH
         ).wait_send()
+
+    barrier = pltpu.get_barrier_semaphore()
+    peers = [at_x(1), at_x(-1), at_y(1), at_y(-1), at_y(2), at_z(1), at_z(-1), partner]
+    for peer in peers:
+        pl.semaphore_signal(barrier, inc=1, device_id=peer, device_id_type=MESH)
 
     loads = [
         pltpu.make_async_copy(src, dst, load_sem.at[i])
@@ -96,10 +106,6 @@
     for copy in loads:
         copy.start()
 
-    barrier = pltpu.get_barrier_semaphore()
-    peers = [at_x(1), at_x(-1), at_y(1), at_y(-1), at_y(2), at_z(1), at_z(-1), partner]
-    for peer in peers:
-        pl.semaphore_signal(barrier, inc=1, device_id=peer, device_id_type=MESH)
     pl.semaphore_wait(barrier, len(peers))
 
     SIDES = ((0, 1), (1, -1))
@@ -115,69 +121,59 @@
     def cot_direct(k):
         cols = columns(ZSTEPS[k])
         for d, s in SIDES:
-            send(cot_h.at[:, cols], cot.at[cot_rows(0), cols], 0, cd_r.at[d, k], at_x(s))
+            send(cot_h.at[:, cols], cot.at[cot_rows(0), cols], 0, cd_r.at[k], at_x(s))
 
     def cot_forward(k):
         cols = columns(ZSTEPS[k])
+        arrived(full.at[:, 0], cd_r.at[k])
         for d, s in SIDES:
-            block = cot.at[cot_rows(-s), cols]
-            arrived(block, cd_r.at[d, k])
             part = cot.at[cot_rows(-s, d * half, half), cols]
-            send(part, part, 1, cf_r.at[d, k], at_x(s))
-        if k + 2 < NZ:
-            cot_direct(k + 2)
+            send(part, part, 1, cf_r.at[k], at_x(s))
+        for ahead in AHEAD[k]:
+            cot_direct(ahead)
 
     def cot_done(k):
-        cols = columns(ZSTEPS[k])
-        for d, s in SIDES:
-            part = cot.at[cot_rows(2, d * half, half), cols]
-            arrived(part, cf_r.at[d, k])
+        arrived(pre.at[:, 0], cf_r.at[k])
 
     def w_block(zs, ys):
         return wt.at[dz(zs) * NY + dy(ys), c]
 
-    def w_along_z(s):
+    def w_along_z(s, h):
         for d, step in SIDES:
-            block = w_block(-step * (s - 1), 0)
-            if s == 4:
-                block = block.at[pl.ds(d * hrow, hrow)]
-            send(block, block, 2, wz_r.at[d, s - 1], at_z(step))
+            if s < 4 or d == h:
+                part = w_block(-step * (s - 1), 0).at[pl.ds(h * hrow, hrow)]
+                send(part, part, 2, wz_r.at[s - 1, h], at_z(step))
 
     def w_along_y(j):
         block = w_block(WSTEPS[j], 0)
         for d, step in SIDES:
-            send(block, block, 3, wy_r.at[d, j], at_y(step))
-
-    def w_z(s):
+            send(block, block, 3, wy_r.at[j], at_y(step))
+
+    def w_z(s, h):
+        arrived(wt.at[0, 0] if s < 4 else wt.at[0, 0, pl.ds(0, hrow)], wz_r.at[s - 1, h])
+        if s < 4:
+            w_along_z(s + 1, h)
+        if h == 1:
+            for j in (2 * s - 1, 2 * s) if s < 4 else (7,):
+                w_along_y(j)
+
+    def w_y(j):
+        arrived(wt.at[0], wy_r.at[j])
         for d, step in SIDES:
-            block = w_block(-step * s, 0)
-            if s == 4:
-                block = block.at[pl.ds(d * hrow, hrow)]
-            arrived(block, wz_r.at[d, s - 1])
-        if s < 4:
-            w_along_z(s + 1)
-            w_along_y(2 * s - 1)
-            w_along_y(2 * s)
-        else:
-            w_along_y(7)
-
-    def w_y(j):
-        for d, step in SIDES:
-            block = w_block(WSTEPS[j], -step)
-            arrived(block, wy_r.at[d, j])
-            part = block.at[pl.ds(d * hrow, hrow)]
-            send(part, part, 4, wf_r.at[d, j], at_y(step))
+            part = w_block(WSTEPS[j], -step).at[pl.ds(d * hrow, hrow)]
+            send(part, part, 4, wf_r.at[j], at_y(step))
 
     def w_core(j):
-        for d, step in SIDES:
-            part = w_block(WSTEPS[j], 2).at[pl.ds(d * hrow, hrow)]
-            arrived(part, wf_r.at[d, j])
+        arrived(wt.at[0, 0], wf_r.at[j])
         rows = wt.at[pl.ds(dz(WSTEPS[j]) * NY, NY), c]
         send(rows, rows, 5, wd_r.at[j], partner)
 
     def w_done(j):
         rows = wt.at[pl.ds(dz(WSTEPS[j]) * NY, NY), 1 - c]
         arrived(rows, wd_r.at[j])
+
+    def alone(run):
+        pl.when(f >= 0)(run)
 
     def over_rows(first, size, body):
         def step(i, carry):
@@ -202,10 +198,14 @@
 
     def grad(k):
         cot_done(k)
-        part = lax.dot_general(
-            cot[:, columns(ZSTEPS[k])], eh[...], (((0,), (0,)), ((), ())), preferred_element_type=F32
-        )
-        gbuf[k] = part.astype(BF16).reshape(NY, NC, ROWS, part.shape[1])
+
+        @alone
+        def _():
+            part = lax.dot_general(
+                cot[:, columns(ZSTEPS[k])], eh[...], (((0,), (0,)), ((), ())), preferred_element_type=F32
+            )
+            gbuf[k] = part.astype(BF16).reshape(NY, NC, ROWS, part.shape[1])
+
         send(gbuf.at[k, :, 1 - c], precv.at[k], 6, gp_r.at[k], partner)
 
     def pair_done(k):
@@ -219,7 +219,7 @@
 
     CHAIN = (
         ((0, -1), (0, 0), *((k, r) for k in (1, 3, 5) for r in (2, 1, -1, 0))),
-        ((0, 2), (0, 1), *((k, r) for k in (2, 4, 6) for r in (-1, 2, 1, 0))),
+        ((0, 2), (0, 1), (2, -1), (2, 2), (2, 1), (2, 0), (4, 2), (4, -1), (4, 1), (4, 0), (6, 2), (6, 1), (6, -1), (6, 0)),
     )
 
     def chain_before(d, k, r):
@@ -237,45 +237,56 @@
         send(gbuf.at[k, dy(r), c], zrecv.at[d, i], 7, gz_r.at[d, i], at_z(SIDES[d][1]))
 
     def own_sum(i):
-        r = (1, -1, 2)[i]
+        r = (2, 1, -1)[i]
         gbuf[7, dy(r), c] = add_up(7, r, chain_before(0, 7, r) + chain_before(1, 7, r)).astype(BF16)
-        send(gbuf.at[7, dy(r), c], yrecv.at[i], 8, gy_r.at[i], at_y(r))
+        send(gbuf.at[7, dy(r), c], yrecv.at[i], 8, gy_r.at[0], at_y(r))
 
     def grad_end():
         total = add_up(7, 0, chain_before(0, 7, 0) + chain_before(1, 7, 0))
+        arrived(yrecv, gy_r.at[0])
         for i in range(3):
-            arrived(yrecv.at[i], gy_r.at[i])
             total += yrecv[i].astype(F32)
         gsum[...] += total
 
     def partial(j):
         w_done(j)
-        rows = wt[pl.ds(dz(WSTEPS[j]) * NY, NY)].reshape(WIDE, wt.shape[3])
-        part = lax.dot_general(lg[...], rows, (((1,), (1,)), ((), ())), preferred_element_type=F32)
-        pbuf[j] = part.astype(BF16).reshape(NX, xrows, WIDE)
+
+        @alone
+        def _():
+            at = pl.ds(dz(WSTEPS[j]) * NY, NY)
+
+            def product(cols, sign):
+                rows = sign * wt[at, :, :, cols].reshape(WIDE, -1)
+                return lax.dot_general(lg[:, cols], rows, (((1,), (1,)), ((), ())), preferred_element_type=F32)
+
+            part = product(slice(0, KCUT), 1) - product(slice(KCUT, None), -1)
+            pbuf[j] = part.astype(BF16).reshape(NX, xrows, WIDE)
+
         for d, s in SIDES:
-            send(pbuf.at[j, dx(2), pl.ds(d * half, half)], pre.at[d, j], 9, mp_r.at[d, j], at_x(s))
+            send(pbuf.at[j, dx(2), pl.ds(d * half, half)], pre.at[d, j], 9, mp_r.at[j], at_x(s))
 
     def partial_on(j):
+        arrived(pre.at[:, 0], mp_r.at[j])
         for d, s in SIDES:
-            arrived(pre.at[d, j], mp_r.at[d, j])
             rows = pl.ds(d * half, half)
             pbuf[j, dx(s), rows] = (pbuf[j, dx(s), rows].astype(F32) + pre[d, j].astype(F32)).astype(BF16)
-            send(pbuf.at[j, dx(s)], full.at[d, j], 10, mf_r.at[d, j], at_x(s))
+            send(pbuf.at[j, dx(s)], full.at[d, j], 10, mf_r.at[j], at_x(s))
 
     def partial_end(j):
-        total = pbuf[j, x].astype(F32)
-        for d, s in SIDES:
-            arrived(full.at[d, j], mf_r.at[d, j])
-            total += full[d, j].astype(F32)
-        cols = columns(WSTEPS[j])
-        mixed[:, cols] = total.astype(BF16)
-
-    def hidden(m):
+        arrived(full.at[:, 0], mf_r.at[j])
+        total = pbuf[j, x].astype(F32) + full[0, j].astype(F32) + full[1, j].astype(F32)
+        mixed[:, columns(WSTEPS[j])] = total.astype(BF16)
+
+    def hidden(m, i):
         rows = pl.ds(m * xrows, xrows)
-        hc[...] = jnp.dot(
-            cot[rows, :], wt[...].reshape(NZ * WIDE, wt.shape[3]), preferred_element_type=F32
-        )
+        cols = (slice(0, CUT), slice(CUT, None))[i]
+
+        @alone
+        def _():
+            hc[:, cols] = jnp.dot(
+                cot[rows, :], wt[:, :, :, cols].reshape(NZ * WIDE, -1), preferred_element_type=F32
+            )
+
 
     def pointwise(m):
         def body(rows):
@@ -291,7 +302,8 @@
     def begin():
         cot_direct(0)
         loads[3].wait()
-        w_along_z(1)
+        w_along_z(1, 0)
+        w_along_z(1, 1)
         w_along_y(0)
         cot_direct(1)
         loads[0].wait()
@@ -333,6 +345,21 @@
         all_sent(kind, like)
 
 
+def put_kernel(*refs):
+    *refs, sem = refs
+    half = len(refs) // 2
+    copies = []
+    for src, dst in zip(refs[:half], refs[half:]):
+        rows = src.shape[0] // PARTS
+        for i in range(PARTS):
+            at = pl.ds(i * rows, rows)
+            copies.append(pltpu.make_async_copy(src.at[at], dst.at[at], sem.at[len(copies)]))
+    for copy in copies:
+        copy.start()
+    for copy in copies:
+        copy.wait()
+
+
 def on_device(lg, lu, eg, eu, cot, weight, running):
     tokens, block = lg.shape
     xrows, width = cot.shape
@@ -361,23 +388,33 @@
             vmem((xrows, block), F32),
             dma((7,)),
             dma((11,)),
-            dma((2, NZ)),
-            dma((2, NZ)),
-            dma((2, 4)),
-            dma((2, NZ)),
-            dma((2, NZ)),
+            dma((NZ,)),
+            dma((NZ,)),
+            dma((4, 2)),
+            dma((NZ,)),
+            dma((NZ,)),
             dma((NZ,)),
             dma((NZ,)),
             dma((2, 14)),
-            dma((3,)),
-            dma((2, NZ)),
-            dma((2, NZ)),
+            dma((1,)),
+            dma((NZ,)),
+            dma((NZ,)),
         ],
         compiler_params=pltpu.CompilerParams(
             collective_id=0, has_side_effects=True, vmem_limit_bytes=52 * 1024 * 1024
         ),
         name="layer",
     )(lg, lu, eg, eu, cot, weight.T, running.T)
+    results = (gate_grad, up_grad, mixed, total)
+    gate_grad, up_grad, mixed, total = pl.pallas_call(
+        put_kernel,
+        out_shape=[jax.ShapeDtypeStruct(v.shape, v.dtype) for v in results],
+        in_specs=[pl.BlockSpec(memory_space=vmem)] * 4,
+        out_specs=[pl.BlockSpec(memory_space=pl.ANY)] * 4,
+        scratch_shapes=[dma((4 * PARTS,))],
+        compiler_params=pltpu.CompilerParams(vmem_limit_bytes=1 << 20),
+        name="put",
+    )(*results)
     return (mixed, gate_grad, up_grad, total.T)
 
 

time: 61 us -> 58.1 us (0.952)
  local copies, waits for them, and re-layouts: 3.94 us -> 0 us
  Pallas kernels: 56.3 us -> 57.2 us
    unnamed x4 -> x0, local copies, waits for them, and re-layouts: 3.94 us -> none
    pallas_call x0 -> x1, Pallas kernels: none -> 2.14 us  [on_device(): pl.pallas_call(put_kernel, out_shape=[jax.ShapeDtypeStruct(v.shape, v.dty...]
    pallas_call x1, Pallas kernels: 56.3 us -> 55.1 us  [on_device(): pl.pallas_call(kernel, out_shape=(vmem((xrows, width), BF16), vmem((token...]
where the time goes in v3:
time: 58.1 us; the launch traced here: 58 us
  Pallas kernels  57.2 us (98%)
  between operations  0.8 us (1%)
    pallas_call x1, Pallas kernels, on_device(): pl.pallas_call(kernel, out_shape=(vmem((xrows, width), BF16), vmem((token...  55.1 us
    pallas_call x1, Pallas kernels, on_device(): pl.pallas_call(put_kernel, out_shape=[jax.ShapeDtypeStruct(v.shape, v.dty...  2.14 us

profile of v3, /device:TPU:1, one launch (start us, length us, event | category | flops | bytes accessed | tf_op | source)
XLA Modules:
  0.0 58.0 jit_solution(18420272138616715857)
XLA Ops:
  0.6 55.1 %layer.1 = (bf16[160,2048]{1,0:T(8,128)(2,1)S(1)}, bf16[640,1408]{1,0:T(8,128)(2,1)S(1)}, bf16[640,1408]{1,0:T(8,128)(2,1)S(1)}, f32[32,1408]{1,0:T(8,128)S(1)}) custom-call(bf16[640,1408]{1,0:T(8,128)(2,1)} %lg_h.1, bf16[640,1408]{1,0:T(8,128)(2,1)} %lu_h.1, bf16[640,1408]{1,0:T(8,128)(2,1)} %eg_h.1, bf16[640,1408]{1,0:T(8,128)(2,1)} %eu_h.1, ...), custom_call_target="tpu_custom_call" | custom-call | tf_op jit(solution)/shard_map/layer/pallas_call | solution.py:367
  55.7 2.1 %put.1 = (bf16[640,1408]{1,0:T(8,128)(2,1)}, bf16[640,1408]{1,0:T(8,128)(2,1)}, bf16[160,2048]{1,0:T(8,128)(2,1)}, f32[32,1408]{1,0:T(8,128)}) custom-call(bf16[640,1408]{1,0:T(8,128)(2,1)S(1)} %get-tuple-element.12.refs_0_, bf16[640,1408]{1,0:T(8,128)(2,1)S(1)} %get-tuple-element.13.refs_1_, bf16[160,2048]{1,0:T(8,128)(2,1)S(1)} %get-tuple-element.14.refs_2_, ...), custom_call_target="tpu_custom_call" | custom-call | tf_op jit(solution)/shard_map/put/pallas_call | solution.py:409

commit v4 on v3

--- a/solution.py
+++ b/solution.py
@@ -13,21 +13,21 @@
 ROWS = 32
 WIDE = NY * NC * ROWS
 TILE = 16
-AHEAD = ((2,), (3,), (4, 5), (6,), (7,), (), (), ())
+AHEAD = ((), (3,), (4,), (5,), (6,), (7,), (), ())
 CUT = 1024
 KCUT = 768
-PARTS = 2
+PARTS = (1, 1, 1, 1)
 
 
 ORDER = (
-    "B", "e0", "e1", "e2", "e3", "c", "L", "l0", "l1", "l2", "z1_0", "l3", "z1_1", "y0", "f0", "f1", "z2_0", "g0",
-    "z2_1", "y1", "f2", "z3_0", "g1", "d0", "u0", "u1", "v0", "v1", "y2", "k0", "z3_1", "f3", "z4_0", "g2", "d1",
-    "u2", "u3", "y3", "f4", "p0", "u4", "y4", "d2", "v2", "v3", "k1", "f5", "k2", "u5", "v4", "v5", "g3", "z4_1",
-    "p1", "f6", "y5", "p2", "g4", "d3", "u6", "y6", "u7", "f7", "k3", "q0", "d4", "v6", "u8", "v7", "k4", "g5", "v8",
-    "q1", "p3", "u9", "y7", "p4", "v9", "k5", "g6", "d5", "u10", "q2", "k6", "g7", "p5", "u11", "k7", "r0", "d6",
-    "v10", "p6", "r1", "d7", "u12", "p7", "v11", "v12", "q3", "h0_0", "u13", "q4", "h0_1", "v13", "w0", "r2", "h1_0",
-    "q5", "h1_1", "o0", "q6", "w1", "h2_0", "q7", "h2_1", "o1", "w2", "r3", "h3_0", "o2", "h3_1", "w3", "r4", "r5",
-    "r6", "G", "r7",
+    "B", "e0", "e1", "e2", "e3", "c", "L", "l0", "l1", "l2", "l3", "z1_0", "z1_1", "y0", "f0", "f1", "z2_0", "f2",
+    "z2_1", "y1", "g0", "g1", "z3_0", "y2", "z3_1", "f3", "k0", "d0", "u0", "u1", "v0", "v1", "g2", "d1", "u2", "u3",
+    "y3", "z4_0", "f4", "p0", "z4_1", "g3", "d2", "v2", "y4", "u4", "k1", "v3", "f5", "k2", "g4", "d3", "u5", "v4",
+    "v5", "f6", "p1", "u6", "y5", "q0", "d4", "g5", "u7", "y6", "k3", "v6", "v7", "f7", "p2", "g6", "d5", "u8", "v8",
+    "q1", "y7", "p3", "k4", "u9", "k5", "v9", "r0", "d6", "k6", "g7", "u10", "v10", "q2", "k7", "p4", "p5", "u11",
+    "p6", "d7", "r1", "q3", "p7", "u12", "h0_0", "v11", "v12", "r2", "h0_1", "w0", "u13", "q4", "v13", "h1_0", "q5",
+    "h1_1", "q6", "w1", "o0", "h2_0", "r3", "h2_1", "w2", "o1", "q7", "h3_0", "h3_1", "w3", "o2", "r4", "r5", "r6",
+    "G", "r7",
 )
 
 
@@ -306,6 +306,7 @@
         w_along_z(1, 1)
         w_along_y(0)
         cot_direct(1)
+        cot_direct(2)
         loads[0].wait()
         loads[1].wait()
 
@@ -349,9 +350,9 @@
     *refs, sem = refs
     half = len(refs) // 2
     copies = []
-    for src, dst in zip(refs[:half], refs[half:]):
-        rows = src.shape[0] // PARTS
-        for i in range(PARTS):
+    for src, dst, parts in zip(refs[:half], refs[half:], PARTS):
+        rows = src.shape[0] // parts
+        for i in range(parts):
             at = pl.ds(i * rows, rows)
             copies.append(pltpu.make_async_copy(src.at[at], dst.at[at], sem.at[len(copies)]))
     for copy in copies:
@@ -411,7 +412,7 @@
         out_shape=[jax.ShapeDtypeStruct(v.shape, v.dtype) for v in results],
         in_specs=[pl.BlockSpec(memory_space=vmem)] * 4,
         out_specs=[pl.BlockSpec(memory_space=pl.ANY)] * 4,
-        scratch_shapes=[dma((4 * PARTS,))],
+        scratch_shapes=[dma((sum(PARTS),))],
         compiler_params=pltpu.CompilerParams(vmem_limit_bytes=1 << 20),
         name="put",
     )(*results)

time: 58.1 us -> 57.5 us (0.990)
  Pallas kernels: 57.2 us -> 56.6 us
    pallas_call x1, Pallas kernels: 55.1 us -> 54.5 us  [on_device(): pl.pallas_call(kernel, out_shape=(vmem((xrows, width), BF16), vmem((token...]
where the time goes in v4:
time: 57.5 us; the launch traced here: 57.4 us
  Pallas kernels  56.6 us (98%)
  between operations  0.8 us (1%)
    pallas_call x1, Pallas kernels, on_device(): pl.pallas_call(kernel, out_shape=(vmem((xrows, width), BF16), vmem((token...  54.5 us
    pallas_call x1, Pallas kernels, on_device(): pl.pallas_call(put_kernel, out_shape=[jax.ShapeDtypeStruct(v.shape, v.dty...  2.11 us

profile of v4, /device:TPU:1, one launch (start us, length us, event | category | flops | bytes accessed | tf_op | source)
XLA Modules:
  0.0 57.4 jit_solution(11226295388527780202)
XLA Ops:
  0.6 54.5 %layer.1 = (bf16[160,2048]{1,0:T(8,128)(2,1)S(1)}, bf16[640,1408]{1,0:T(8,128)(2,1)S(1)}, bf16[640,1408]{1,0:T(8,128)(2,1)S(1)}, f32[32,1408]{1,0:T(8,128)S(1)}) custom-call(bf16[640,1408]{1,0:T(8,128)(2,1)} %lg_h.1, bf16[640,1408]{1,0:T(8,128)(2,1)} %lu_h.1, bf16[640,1408]{1,0:T(8,128)(2,1)} %eg_h.1, bf16[640,1408]{1,0:T(8,128)(2,1)} %eu_h.1, ...), custom_call_target="tpu_custom_call" | custom-call | tf_op jit(solution)/shard_map/layer/pallas_call | solution.py:368
  55.1 2.1 %put.1 = (bf16[640,1408]{1,0:T(8,128)(2,1)}, bf16[640,1408]{1,0:T(8,128)(2,1)}, bf16[160,2048]{1,0:T(8,128)(2,1)}, f32[32,1408]{1,0:T(8,128)}) custom-call(bf16[640,1408]{1,0:T(8,128)(2,1)S(1)} %get-tuple-element.12.refs_0_, bf16[640,1408]{1,0:T(8,128)(2,1)S(1)} %get-tuple-element.13.refs_1_, bf16[160,2048]{1,0:T(8,128)(2,1)S(1)} %get-tuple-element.14.refs_2_, ...), custom_call_target="tpu_custom_call" | custom-call | tf_op jit(solution)/shard_map/put/pallas_call | solution.py:410

commit v5 on v4

--- a/solution.py
+++ b/solution.py
@@ -222,19 +222,26 @@
         ((0, 2), (0, 1), (2, -1), (2, 2), (2, 1), (2, 0), (4, 2), (4, -1), (4, 1), (4, 0), (6, 2), (6, 1), (6, -1), (6, 0)),
     )
 
+    def chain_sem(d, i):
+        k, r = CHAIN[d][i]
+        return gz_r.at[CHAIN[0].index((5, r)) if k == 6 else 14 * d + i]
+
     def chain_before(d, k, r):
         nearer = ((1, 3, 5, 7), (2, 4, 6, 7))[d]
         before = (((0,) + nearer)[nearer.index(k)], r) if k in nearer else None
         if before not in CHAIN[d]:
             return []
         i = CHAIN[d].index(before)
-        arrived(zrecv.at[d, i], gz_r.at[d, i])
+        if k < 7:
+            arrived(zrecv.at[d, i], chain_sem(d, i))
+        elif d == 0:
+            arrived(wt.at[0], chain_sem(d, i))
         return [(d, i)]
 
     def chain(d, i):
         k, r = CHAIN[d][i]
         gbuf[k, dy(r), c] = add_up(k, r, chain_before(d, k, r)).astype(BF16)
-        send(gbuf.at[k, dy(r), c], zrecv.at[d, i], 7, gz_r.at[d, i], at_z(SIDES[d][1]))
+        send(gbuf.at[k, dy(r), c], zrecv.at[d, i], 7, chain_sem(d, i), at_z(SIDES[d][1]))
 
     def own_sum(i):
         r = (2, 1, -1)[i]
@@ -355,8 +362,8 @@
         for i in range(parts):
             at = pl.ds(i * rows, rows)
             copies.append(pltpu.make_async_copy(src.at[at], dst.at[at], sem.at[len(copies)]))
-    for copy in copies:
-        copy.start()
+    for i, copy in enumerate(copies):
+        copy.start(priority=i % 2)
     for copy in copies:
         copy.wait()
 
@@ -396,7 +403,7 @@
             dma((NZ,)),
             dma((NZ,)),
             dma((NZ,)),
-            dma((2, 14)),
+            dma((24,)),
             dma((1,)),
             dma((NZ,)),
             dma((NZ,)),

time: 57.5 us -> 57.5 us (level)
  no operation moved by 1% of the time
where the time goes in v5:
time: 57.5 us; the launch traced here: 57.4 us
  Pallas kernels  56.6 us (98%)
  between operations  0.8 us (1%)
    pallas_call x1, Pallas kernels, on_device(): pl.pallas_call(kernel, out_shape=(vmem((xrows, width), BF16), vmem((token...  54.5 us
    pallas_call x1, Pallas kernels, on_device(): pl.pallas_call(put_kernel, out_shape=[jax.ShapeDtypeStruct(v.shape, v.dty...  2.11 us

profile of v5, /device:TPU:1, one launch (start us, length us, event | category | flops | bytes accessed | tf_op | source)
XLA Modules:
  0.0 57.4 jit_solution(14760182801453312045)
XLA Ops:
  0.6 54.5 %layer.1 = (bf16[160,2048]{1,0:T(8,128)(2,1)S(1)}, bf16[640,1408]{1,0:T(8,128)(2,1)S(1)}, bf16[640,1408]{1,0:T(8,128)(2,1)S(1)}, f32[32,1408]{1,0:T(8,128)S(1)}) custom-call(bf16[640,1408]{1,0:T(8,128)(2,1)} %lg_h.1, bf16[640,1408]{1,0:T(8,128)(2,1)} %lu_h.1, bf16[640,1408]{1,0:T(8,128)(2,1)} %eg_h.1, bf16[640,1408]{1,0:T(8,128)(2,1)} %eu_h.1, ...), custom_call_target="tpu_custom_call" | custom-call | tf_op jit(solution)/shard_map/layer/pallas_call | solution.py:375
  55.1 2.1 %put.1 = (bf16[640,1408]{1,0:T(8,128)(2,1)}, bf16[640,1408]{1,0:T(8,128)(2,1)}, bf16[160,2048]{1,0:T(8,128)(2,1)}, f32[32,1408]{1,0:T(8,128)}) custom-call(bf16[640,1408]{1,0:T(8,128)(2,1)S(1)} %get-tuple-element.12.refs_0_, bf16[640,1408]{1,0:T(8,128)(2,1)S(1)} %get-tuple-element.13.refs_1_, bf16[160,2048]{1,0:T(8,128)(2,1)S(1)} %get-tuple-element.14.refs_2_, ...), custom_call_target="tpu_custom_call" | custom-call | tf_op jit(solution)/shard_map/put/pallas_call | solution.py:417
